TPU v7x, 32 devices: a whole 2x2x4 slice. The times are simulated.
32 devices in a mesh: sp: 16 (over z, y, x), tp: 2 (over core).
Axes of the slice: x: 2, y: 2, z: 4, core: 2. Of those that a mesh axis runs over, the one named last changes fastest.
Arguments:
- residual: bfloat16 [4096, 2048], P(('sp', 'tp')), may hold values from -6 to 6
- queries: bfloat16 [4096, 1152], P('sp', 'tp'), may hold values from -800 to 800
- latent: bfloat16 [4096, 256], P('sp'), may hold values from -6 to 6
- rope_key: bfloat16 [4096, 32], P('sp'), may hold values from -6 to 6
- doc_ids: int32 [4096], P('sp'), may hold values from 0 to 5, never falling along the last dimension, each value on 1 to 2048 neighbouring positions
- latent_to_key: bfloat16 [256, 768], P(None, 'tp'), may hold values from -0.375 to 0.375
- latent_to_value: bfloat16 [256, 768], P(None, 'tp'), may hold values from -0.375 to 0.375
- out_proj: bfloat16 [768, 2048], replicated, may hold values from -0.21875 to 0.21875
- mix_gain: float32 [2048], replicated, may hold values from 0.1 to 1.9
- moe_gain: float32 [2048], replicated, may hold values from 0.1 to 1.9
- expert_ids: int32 [4096, 2], P(('sp', 'tp')), may hold values from 0 to 15, as said below
- route_weight: float32 [4096, 2], P(('sp', 'tp')), may hold values from 0.1 to 1
- gate_weight: bfloat16 [16, 2048, 1024], P('sp', None, 'tp'), may hold values from -0.125 to 0.125
- up_weight: bfloat16 [16, 2048, 1024], P('sp', None, 'tp'), may hold values from -0.125 to 0.125
- down_weight: bfloat16 [16, 1024, 2048], P('sp', 'tp'), may hold values from -0.1875 to 0.1875
Outputs:
- output: bfloat16 [4096, 2048], P(('sp', 'tp'))
Inputs may be any that keep to these rules, and one draw needn't show every extreme that they name: `expert_ids`: each row names 2 different experts of one group of 4 consecutive numbers; in each aligned block of 128 rows (the rows of one device) no expert is named more than 32 times, and some expert exactly 32 times.
All inputs are finite; a program needn't handle non-finite values.
Results may differ from a plain program's by a relative error of at most 0.013.
Values may be sent and summed in bfloat16 or wider, within the bound.
A program may use at most 64 MiB of HBM per device.

v0:
```python
import functools
import math

import jax
import jax.numpy as jnp
from jax import lax
from jax.experimental import pallas as pl
from jax.experimental.pallas import tpu as pltpu
from jax.sharding import PartitionSpec as P

UNROTATED_DIM = 64
ROPE = 32
VALUE_ENTRIES = 64
GROUPS = 4
HEAD_LANES = 128
MESH = pl.DeviceIdType.MESH

rope_base = 10000.0
epsilon = 1e-06


def angles_of(positions):
    half_width = ROPE // 2
    frequency = rope_base ** (-jnp.arange(half_width, dtype=jnp.float32) / half_width)
    angles = frequency[:, None] * positions.astype(jnp.float32)[None, :]
    return jnp.cos(angles), jnp.sin(angles)


def rms_scale(source, gain):
    return source * lax.rsqrt(jnp.mean(source * source, axis=-1, keepdims=True) + epsilon) * gain


def turn(pair, cosine, sine):
    half = ROPE // 2
    upper, lower = pair[:half].astype(jnp.float32), pair[half:].astype(jnp.float32)
    return jnp.concatenate(
        [upper * cosine - lower * sine, lower * cosine + upper * sine], axis=0
    ).astype(jnp.bfloat16)


def greet(groups, plane, meanwhile=None):
    index, core = lax.axis_index("sp"), lax.axis_index("tp")
    level, place = index // plane, lax.rem(index, plane)
    barrier = pltpu.get_barrier_semaphore()
    peers = [(lax.rem(level + d, groups) * plane + place, core) for d in range(1, groups)]
    peers += [(level * plane + lax.rem(place + d, plane), core) for d in range(1, plane)]
    peers += [(index, 1 - core)]
    for peer in peers:
        pl.semaphore_signal(barrier, inc=1, device_id=peer, device_id_type=MESH)
    if meanwhile is not None:
        meanwhile(index, core)
    pl.semaphore_wait(barrier, len(peers))
    return index, core, level, place


def remote(source, target, send_sem, recv_sem, peer):
    return pltpu.make_async_remote_copy(
        src_ref=source, dst_ref=target, send_sem=send_sem, recv_sem=recv_sem,
        device_id=peer, device_id_type=MESH,
    )


def level_order(groups):
    return sorted(range(groups), key=lambda d: min(d, groups - d))


def nearest(level, groups, at):
    picked = 0
    for l in range(groups):
        choice = sorted(range(groups), key=lambda s: (abs(s - l), s))[at]
        picked = picked + jnp.where(level == l, choice, 0)
    return picked


def expert_kernel(
    groups, plane, capacity, rows_ref, meta_ref, gate_ref, up_ref, down_ref, out_ref,
    gate, up, down, metas, landed, spread, arrived, hidden, partial, passed, mixed, back, merged,
    w_sem, m_send, m_recv, z_send, z_recv, p_send, p_recv, own_sem, t_send, t_recv,
    x_send, x_recv, b_send, b_recv, keep_sem, r_send, r_recv,
):
    weights = [
        pltpu.make_async_copy(source, target, w_sem.at[i])
        for i, (source, target) in enumerate([(gate_ref, gate), (up_ref, up), (down_ref, down)])
    ]
    for copy in weights:
        copy.start()
    index, core, level, place = greet(groups, plane)
    started = []
    slots = plane * capacity
    group_rows = rows_ref.shape[1]
    width = rows_ref.shape[2]
    source_of = [nearest(level, groups, k) for k in range(groups)]

    def begin(copy):
        copy.start()
        started.append(copy)

    for k in range(1, groups):
        other = source_of[k]
        peer = (other * plane + place, core)
        begin(remote(meta_ref.at[other], metas.at[level], m_send.at[k], m_recv.at[level], peer))
        begin(remote(rows_ref.at[other], landed.at[level], z_send.at[k], z_recv.at[level], peer))
    metas[level] = meta_ref[level]

    def send_out(k):
        source = source_of[k]
        if k == 0:
            rows = rows_ref[level]
        else:
            peer = (source * plane + place, core)
            remote(meta_ref.at[source], metas.at[source], m_send.at[k], m_recv.at[source], peer).wait_recv()
            remote(rows_ref.at[source], landed.at[source], z_send.at[k], z_recv.at[source], peer).wait_recv()
            rows = landed[source]
        info = metas[source][:, :group_rows].astype(jnp.float32)
        slot = lax.broadcasted_iota(jnp.int32, (slots, group_rows), 0).astype(jnp.float32)
        chooser = jnp.where((slot == info[0:1]) | (slot == info[1:2]), 1.0, 0.0)
        picked = jnp.dot(chooser.astype(jnp.bfloat16), rows, preferred_element_type=jnp.float32)
        for e in range(plane):
            spread[k, e] = picked[e * capacity : (e + 1) * capacity].astype(jnp.bfloat16)
        for far in range(plane - 1, 0, -1):
            to = lax.rem(place + far, plane)
            begin(remote(
                spread.at[k, to], arrived.at[k, core, place],
                p_send.at[k * plane + far], p_recv.at[k * plane + place],
                (level * plane + to, core),
            ))
        pltpu.make_async_copy(
            spread.at[k, place], arrived.at[k, core, place], own_sem.at[k]
        ).start()

    def hand_over(k):
        for far in range(plane):
            origin = lax.rem(place + plane - far, plane)
            if far:
                remote(
                    spread.at[k, origin], arrived.at[k, core, origin],
                    p_send.at[k * plane + far], p_recv.at[k * plane + origin],
                    (level * plane + origin, core),
                ).wait_recv()
            else:
                pltpu.make_async_copy(
                    spread.at[k, place], arrived.at[k, core, place], own_sem.at[k]
                ).wait()
            begin(remote(
                arrived.at[k, core, origin], arrived.at[k, core, origin],
                t_send.at[k * plane + far], t_recv.at[k * plane + origin], (index, 1 - core),
            ))

    def experts(k):
        for origin in range(plane):
            remote(
                arrived.at[k, 1 - core, origin], arrived.at[k, 1 - core, origin],
                t_send.at[k * plane], t_recv.at[k * plane + origin], (index, 1 - core),
            ).wait_recv()
        units = gate.shape[1]
        unit_tile = math.gcd(units, 256)
        tile = math.gcd(width, 256)

        def hide(j, carry):
            columns = pl.ds(pl.multiple_of(j * unit_tile, unit_tile), unit_tile)
            rows = arrived[k].reshape(2 * slots, width)
            gated = jnp.dot(rows, gate[:, columns], preferred_element_type=jnp.float32)
            raised = jnp.dot(rows, up[:, columns], preferred_element_type=jnp.float32)
            hidden[:, columns] = (gated / (1.0 + jnp.exp(-gated)) * raised).astype(jnp.bfloat16)
            return carry

        lax.fori_loop(0, units // unit_tile, hide, 0)

        def lower(j, carry):
            columns = pl.ds(pl.multiple_of(j * tile, tile), tile)
            piece = jnp.dot(hidden[...], down[:, columns], preferred_element_type=jnp.float32)
            partial[k, :, :, :, columns] = piece.reshape(2, plane, capacity, tile).astype(jnp.bfloat16)
            return carry

        lax.fori_loop(0, width // tile, lower, 0)
        begin(remote(
            partial.at[k, 1 - core], passed.at[k], x_send.at[k], x_recv.at[k], (index, 1 - core)
        ))

    def send_back(k):
        remote(
            partial.at[k, core], passed.at[k], x_send.at[k], x_recv.at[k], (index, 1 - core)
        ).wait_recv()
        for e in range(plane):
            mixed[k, e] = (
                partial[k, core, e].astype(jnp.float32) + passed[k, e].astype(jnp.float32)
            ).astype(jnp.bfloat16)
        for far in range(plane - 1, 0, -1):
            to = lax.rem(place + far, plane)
            begin(remote(
                mixed.at[k, to], back.at[k, place],
                b_send.at[k * plane + far], b_recv.at[k * plane + place],
                (level * plane + to, core),
            ))
        pltpu.make_async_copy(mixed.at[k, place], back.at[k, place], keep_sem.at[k]).start()

    def combine(k):
        source = source_of[k]
        for far in range(1, plane):
            origin = lax.rem(place + plane - far, plane)
            remote(
                mixed.at[k, origin], back.at[k, origin],
                b_send.at[k * plane + far], b_recv.at[k * plane + origin],
                (level * plane + origin, core),
            ).wait_recv()
        pltpu.make_async_copy(mixed.at[k, place], back.at[k, place], keep_sem.at[k]).wait()
        info = metas[source][:, :group_rows].astype(jnp.float32)
        slot = lax.broadcasted_iota(jnp.int32, (slots, group_rows), 0).astype(jnp.float32)
        hit_first, hit_second = slot == info[0:1], slot == info[1:2]
        returned = back[k].reshape(slots, width)
        result = 0.0
        for term in range(2):
            share = jnp.where(hit_first, info[2 + term : 3 + term], 0.0) + jnp.where(
                hit_second, info[4 + term : 5 + term], 0.0
            )
            result = result + lax.dot_general(
                share.astype(jnp.bfloat16), returned, (((0,), (0,)), ((), ())),
                preferred_element_type=jnp.float32,
            )
        if k == 0:
            out_ref[level] = result.astype(jnp.bfloat16)
        else:
            merged[k] = result.astype(jnp.bfloat16)
            begin(remote(
                merged.at[k], out_ref.at[level], r_send.at[k], r_recv.at[level],
                (source * plane + place, core),
            ))

    send_out(0)
    send_out(1)
    hand_over(0)
    for copy in weights:
        copy.wait()
    experts(0)
    send_back(0)
    for k in range(1, groups):
        if k + 1 < groups:
            send_out(k + 1)
        hand_over(k)
        experts(k)
        if k > 1:
            combine(k - 1)
        send_back(k)
    combine(groups - 1)
    combine(0)
    for k in range(1, groups):
        other = source_of[k]
        remote(
            merged.at[k], out_ref.at[other], r_send.at[k], r_recv.at[other],
            (other * plane + place, core),
        ).wait_recv()
    for copy in started:
        copy.wait_send()


def run_experts(rows, meta, gate, up, down, plane, capacity):
    groups, group_rows, width = rows.shape
    units = gate.shape[1]
    vmem = pl.BlockSpec(memory_space=pltpu.VMEM)
    hbm = pl.BlockSpec(memory_space=pl.ANY)
    dma = pltpu.SemaphoreType.DMA
    few, many = dma((groups,)), dma((groups * plane,))

    def held(*shape):
        return pltpu.VMEM(shape, jnp.bfloat16)

    block = held(groups, plane, capacity, width)
    double = held(groups, 2, plane, capacity, width)
    return pl.pallas_call(
        functools.partial(expert_kernel, groups, plane, capacity),
        out_shape=jax.ShapeDtypeStruct((groups, group_rows, width), jnp.bfloat16),
        in_specs=[vmem, vmem, hbm, hbm, hbm],
        out_specs=vmem,
        scratch_shapes=[
            held(*gate.shape), held(*up.shape), held(*down.shape), held(*meta.shape),
            held(groups, group_rows, width), block, double,
            held(2 * plane * capacity, units), double, block, block, block,
            held(groups, group_rows, width),
            dma((3,)), few, few, few, few, many, many, few, many, many,
            few, few, many, many, few, few, few,
        ],
        compiler_params=pltpu.CompilerParams(
            collective_id=1, has_side_effects=True, vmem_limit_bytes=48 * 1024 * 1024
        ),
        name="run_experts",
    )(rows, meta, gate, up, down)


def attend_kernel(
    groups, plane, heads,
    query_hbm, latent_hbm, rope_hbm, wk_hbm, wv_hbm, proj_hbm, residual_hbm,
    cos_ref, sin_ref, docs_ref, member_ref, mix_gain_ref, moe_gain_ref,
    middle_ref, grouped_ref,
    query, latent, rope, wk, wv, proj, residual,
    packs, turned, wv_turned, high, total, acc, halves, full, mix, normed,
    load_sem, z_send, z_recv, p_send, p_recv, t_send, t_recv, x_send, x_recv,
):
    loads = [
        pltpu.make_async_copy(source, target, load_sem.at[i])
        for i, (source, target) in enumerate([
            (latent_hbm, latent), (rope_hbm, rope), (query_hbm, query), (wk_hbm, wk),
            (wv_hbm, wv), (residual_hbm, residual), (proj_hbm, proj),
        ])
    ]
    for copy in loads:
        copy.start()
    rows = latent.shape[0]
    half = rows // 2
    per_head = UNROTATED_DIM + ROPE
    cosine, sine = cos_ref[...], sin_ref[...]
    docs = docs_ref[...]

    def pack(index, core):
        loads[0].wait()
        loads[1].wait()
        key = turn(rope[...], cosine, sine)
        for part in range(2):
            span = slice(part * half, (part + 1) * half)
            packs[index, part, :half, :] = latent[span, :]
            line = lax.broadcasted_iota(jnp.int32, (ROPE, half), 0)
            ids = jnp.where(line == 0, jnp.broadcast_to(docs[:, span], (ROPE, half)), 0.0)
            packs[index, part, half:, :half] = key[:, span]
            packs[index, part, half:, half : 2 * half] = ids.astype(jnp.bfloat16)

    index, core, level, place = greet(groups, plane, pack)
    reach = groups // 2

    def z_copy(d):
        return remote(
            packs.at[index, core], packs.at[index, core], z_send.at[d], z_recv.at[d],
            (lax.rem(level + d, groups) * plane + place, core),
        )

    def z_arrival(d):
        block = lax.rem(level + groups - d, groups) * plane + place
        return remote(
            packs.at[block, core], packs.at[block, core], z_send.at[d], z_recv.at[d],
            (block, core),
        )

    def p_copy(d, far):
        block = lax.rem(level + groups - d, groups) * plane + place
        return remote(
            packs.at[block, core], packs.at[block, core], p_send.at[d * plane + far],
            p_recv.at[d * plane + far],
            (level * plane + lax.rem(place + far, plane), core),
        )

    def p_arrival(d, far):
        origin = lax.rem(place + plane - far, plane)
        block = lax.rem(level + groups - d, groups) * plane + origin
        return remote(
            packs.at[block, core], packs.at[block, core], p_send.at[d * plane + far],
            p_recv.at[d * plane + far], (level * plane + origin, core),
        )

    def t_copy(d, far, part):
        origin = lax.rem(place + plane - far, plane)
        block = lax.rem(level + groups - d, groups) * plane + origin
        return remote(
            packs.at[block, part], packs.at[block, part], t_send.at[d * plane + far],
            t_recv.at[d * plane + far], (index, 1 - core),
        )

    def wanted(d, far, sender):
        ahead = lax.rem(place + far, plane) > place if sender else place >= far
        live = level >= d
        if d == 0:
            return live & ahead
        if d == reach:
            return live & jnp.logical_not(ahead)
        return live

    for d in range(1, reach + 1):
        pl.when(level + d < groups)(lambda d=d: z_copy(d).start())
    for far in range(1, plane):
        pl.when(wanted(0, far, True))(lambda far=far: p_copy(0, far).start())

    for copy in loads[2:5]:
        copy.wait()
    blank = jnp.zeros((HEAD_LANES - per_head, rows), jnp.bfloat16)
    for h in range(heads):
        own = query[h * per_head : (h + 1) * per_head, :]
        plain, moved = own[:UNROTATED_DIM], turn(own[UNROTATED_DIM:], cosine, sine)
        parts = [plain, moved, blank] if h % 2 == 0 else [moved, blank, plain]
        turned[h] = jnp.concatenate(parts, axis=0)
    wv_turned[...] = wv[...].astype(jnp.float32).T.astype(jnp.bfloat16)
    power = per_head ** (-0.5) * math.log2(math.e)

    def attend(block, first):
        source = jnp.concatenate([packs[block, part, :half, :] for part in range(2)], axis=0)
        tail = jnp.concatenate(
            [
                jnp.concatenate([packs[block, part, half:, :half] for part in range(2)], axis=1),
                jnp.concatenate(
                    [packs[block, part, half : half + 16, half : 2 * half] for part in range(2)], axis=1
                ),
            ],
            axis=0,
        )
        shape = (ROPE + 16, 3 * HEAD_LANES)
        line = lax.broadcasted_iota(jnp.int32, shape, 0)
        lane = lax.broadcasted_iota(jnp.int32, shape, 1)
        keyed = (line < ROPE) & ((lane == line + UNROTATED_DIM) | (lane == line + 2 * HEAD_LANES))
        named = (line == ROPE) & (lane >= HEAD_LANES) & (lane < 2 * HEAD_LANES)
        chooser = jnp.where(keyed | named, 1.0, 0.0).astype(jnp.bfloat16)
        extra = lax.dot_general(
            tail, chooser, (((0,), (0,)), ((), ())), preferred_element_type=jnp.float32
        )
        extras = [
            extra[:, :HEAD_LANES].astype(jnp.bfloat16), extra[:, 2 * HEAD_LANES :].astype(jnp.bfloat16)
        ]
        theirs = extra[:, HEAD_LANES : 2 * HEAD_LANES]
        theirs = jnp.concatenate([theirs] * (rows // HEAD_LANES), axis=1)
        live = theirs == docs
        if first:
            live = live & (
                lax.broadcasted_iota(jnp.int32, (rows, rows), 0)
                <= lax.broadcasted_iota(jnp.int32, (rows, rows), 1)
            )
        bias = jnp.where(live, 0.0, -1e30)
        keys = jnp.dot(source, wk[...], preferred_element_type=jnp.float32).astype(jnp.bfloat16)
        values = lax.dot_general(
            wv_turned[...], source, (((1,), (1,)), ((), ())), preferred_element_type=jnp.float32
        ).astype(jnp.bfloat16)
        side = lax.broadcasted_iota(jnp.int32, (rows, HEAD_LANES), 1) < UNROTATED_DIM
        for h in range(heads):
            low = h // 2 * HEAD_LANES
            pair = keys[:, low : low + HEAD_LANES]
            key = jnp.where(side, pair, extras[0]) if h % 2 == 0 else jnp.where(side, extras[1], pair)
            scores = jnp.dot(key, turned[h], preferred_element_type=jnp.float32) + bias
            top = jnp.max(scores, axis=0, keepdims=True)
            if not first:
                old = high[h : h + 1, :]
                top = jnp.maximum(old, top)
            weights = jnp.exp2((scores - top) * power)
            mass = jnp.sum(weights, axis=0, keepdims=True)
            mixed = jnp.dot(
                values[h * VALUE_ENTRIES : (h + 1) * VALUE_ENTRIES], weights.astype(jnp.bfloat16),
                preferred_element_type=jnp.float32,
            )
            high[h : h + 1, :] = top
            if first:
                total[h : h + 1, :] = mass
                acc[h] = mixed
            else:
                factor = jnp.exp2((old - top) * power)
                total[h : h + 1, :] = total[h : h + 1, :] * factor + mass
                acc[h] = acc[h] * factor + mixed

    attend(index, True)
    for d in range(1, reach + 1):

        def arrived(d=d):
            z_arrival(d).wait_recv()
            t_copy(d, 0, core).start()

        pl.when(level >= d)(arrived)
        for far in range(1, plane):
            pl.when(wanted(d, far, True))(lambda d=d, far=far: p_copy(d, far).start())

    def where_is(t):
        block = index - t
        d = level - block // plane
        far = lax.rem(place + plane - lax.rem(block, plane), plane)
        return block, d, far

    def pass_on(t):
        block, d, far = where_is(t)

        def passed():
            p_arrival(d, far).wait_recv()
            t_copy(d, far, core).start()

        pl.when(far > 0)(passed)

    last = jnp.minimum(index, reach * plane)
    pl.when(last > 0)(lambda: pass_on(1))

    def step(t, carry):
        pl.when(t < last)(lambda: pass_on(t + 1))
        block, d, far = where_is(t)
        t_copy(d, far, 1 - core).wait_recv()
        attend(block, False)
        return carry

    lax.fori_loop(1, last + 1, step, 0)

    for h in range(heads):
        done = (acc[h] / total[h : h + 1, :]).astype(jnp.bfloat16)
        for part in range(2):
            halves[part, h * VALUE_ENTRIES : (h + 1) * VALUE_ENTRIES, :] = done[:, part * half : (part + 1) * half]
    swap = remote(halves.at[1 - core], full.at[core], x_send, x_recv, (index, 1 - core))
    swap.start()
    full[core] = halves[core]
    loads[5].wait()
    loads[6].wait()
    remote(halves.at[core], full.at[1 - core], x_send, x_recv, (index, 1 - core)).wait_recv()
    width = proj.shape[1]
    tile = math.gcd(width, 512)
    attended = full[...].reshape(proj.shape[0], half).astype(jnp.float32).T.astype(jnp.bfloat16)

    def project(j, carry):
        columns = pl.ds(pl.multiple_of(j * tile, tile), tile)
        mix[:, columns] = jnp.dot(attended, proj[:, columns], preferred_element_type=jnp.float32)
        return carry

    lax.fori_loop(0, width // tile, project, 0)

    def settle(j, carry):
        some = pl.ds(pl.multiple_of(j * 16, 16), 16)
        branch = rms_scale(mix[some, :], mix_gain_ref[...])
        middle = (residual[some, :].astype(jnp.float32) + branch).astype(jnp.bfloat16)
        middle_ref[some, :] = middle
        normed[some, :] = rms_scale(middle.astype(jnp.float32), moe_gain_ref[...]).astype(jnp.bfloat16)
        return carry

    lax.fori_loop(0, half // 16, settle, 0)
    slots = grouped_ref.shape[0]
    chooser = jnp.where(
        lax.broadcasted_iota(jnp.int32, (slots, half), 0) == member_ref[...], 1.0, 0.0
    ).astype(jnp.bfloat16)

    def group(j, carry):
        columns = pl.ds(pl.multiple_of(j * tile, tile), tile)
        grouped_ref[:, columns] = jnp.dot(
            chooser, normed[:, columns], preferred_element_type=jnp.float32
        ).astype(jnp.bfloat16)
        return carry

    lax.fori_loop(0, width // tile, group, 0)

    swap.wait_send()
    for d in range(reach + 1):
        for far in range(0 if d else 1, plane):
            pl.when((level >= d) if far == 0 else wanted(d, far, False))(
                lambda d=d, far=far: t_copy(d, far, core).wait_send()
            )
            if far:
                pl.when(wanted(d, far, True))(lambda d=d, far=far: p_copy(d, far).wait_send())
    for d in range(1, reach + 1):
        pl.when(level + d < groups)(lambda d=d: z_copy(d).wait_send())


def attend(
    queries, latent, rope_key, wk, wv, proj, residual, cosine, sine, docs, member,
    mix_gain, moe_gain, count, slots,
):
    rows, rank = latent.shape
    half = rows // 2
    plane = count // GROUPS
    heads = wk.shape[1] // UNROTATED_DIM
    width = proj.shape[1]
    vmem = pl.BlockSpec(memory_space=pltpu.VMEM)
    hbm = pl.BlockSpec(memory_space=pl.ANY)
    dma = pltpu.SemaphoreType.DMA
    few, many = dma((GROUPS,)), dma((GROUPS * plane,))

    def held(*shape, dtype=jnp.bfloat16):
        return pltpu.VMEM(shape, dtype)

    loaded = (queries.T, latent, rope_key.T, wk, wv, proj, residual)
    return pl.pallas_call(
        functools.partial(attend_kernel, GROUPS, plane, heads),
        out_shape=(
            jax.ShapeDtypeStruct((half, width), jnp.bfloat16),
            jax.ShapeDtypeStruct((slots, width), jnp.bfloat16),
        ),
        in_specs=[hbm] * 7 + [vmem] * 6,
        out_specs=(vmem, vmem),
        scratch_shapes=[held(*array.shape) for array in loaded] + [
            held(count, 2, half + ROPE, rank),
            held(heads, HEAD_LANES, rows),
            held(heads * VALUE_ENTRIES, rank),
            held(heads, rows, dtype=jnp.float32),
            held(heads, rows, dtype=jnp.float32),
            held(heads, VALUE_ENTRIES, rows, dtype=jnp.float32),
            held(2, heads * VALUE_ENTRIES, half),
            held(2, heads * VALUE_ENTRIES, half),
            held(half, width, dtype=jnp.float32),
            held(half, width),
            dma((7,)), few, few, many, many, many, many, dma, dma,
        ],
        compiler_params=pltpu.CompilerParams(
            collective_id=3, has_side_effects=True, vmem_limit_bytes=40 * 1024 * 1024
        ),
        name="attend",
    )(
        *loaded, cosine, sine, docs, member, mix_gain[None, :], moe_gain[None, :],
    )


def local(
    residual,
    queries,
    latent,
    rope_key,
    doc_ids,
    latent_to_key,
    latent_to_value,
    out_proj,
    mix_gain,
    moe_gain,
    expert_ids,
    route_weight,
    gate_weight,
    up_weight,
    down_weight,
):
    local_rows = queries.shape[0]
    positions = lax.axis_index("sp") * local_rows + jnp.arange(local_rows, dtype=jnp.int32)
    cosine, sine = angles_of(positions)
    row_count, width = residual.shape
    top_count = expert_ids.shape[1]
    expert_count = lax.axis_size("sp")
    capacity = row_count // (expert_count // GROUPS)
    plane = expert_count // GROUPS
    group_rows = capacity * plane // top_count
    group_of = expert_ids[:, 0] // plane
    bins = jnp.arange(expert_count + GROUPS, dtype=jnp.int32)[None, :]
    group_bin = group_of[:, None] + expert_count
    named = jnp.any(expert_ids[:, :, None] == bins[None], axis=1) | (group_bin == bins)
    before = jnp.arange(row_count)[:, None] > jnp.arange(row_count)[None, :]
    earlier = jnp.dot(
        before.astype(jnp.bfloat16), named.astype(jnp.bfloat16), preferred_element_type=jnp.float32
    ).astype(jnp.int32)
    slot_rank = jnp.sum(jnp.where(expert_ids[:, :, None] == bins[None], earlier[:, None], 0), axis=2)
    group_rank = jnp.sum(jnp.where(group_bin == bins, earlier, 0), axis=1)
    slots = lax.rem(expert_ids, plane) * capacity + slot_rank
    member = (group_of * group_rows + group_rank)[:, None]
    chooser = (member == jnp.arange(GROUPS * group_rows, dtype=jnp.int32)[None, :]).astype(
        jnp.bfloat16
    )
    coarse = route_weight.astype(jnp.bfloat16)
    fine = (route_weight - coarse.astype(jnp.float32)).astype(jnp.bfloat16)
    fields = jnp.concatenate(
        [
            (slots + 1).astype(jnp.bfloat16),
            jnp.stack([coarse[:, 0], fine[:, 0], coarse[:, 1], fine[:, 1]], axis=1),
        ],
        axis=1,
    )
    fields = jnp.pad(fields, ((0, 0), (0, 16 - fields.shape[1])))
    meta = lax.dot_general(
        fields, chooser, (((0,), (0,)), ((), ())), preferred_element_type=jnp.float32
    )
    meta = meta - (jnp.arange(16) < top_count)[:, None].astype(jnp.float32)
    meta = meta.astype(jnp.bfloat16).reshape(16, GROUPS, group_rows).transpose(1, 0, 2)
    meta = jnp.pad(meta, ((0, 0), (0, 0), (0, -group_rows % 128)))
    middle, grouped = attend(
        queries, latent, rope_key, latent_to_key, latent_to_value, out_proj, residual,
        cosine, sine, doc_ids.astype(jnp.float32)[None, :], member[:, 0][None, :],
        mix_gain, moe_gain, expert_count, GROUPS * group_rows,
    )
    returned = run_experts(
        grouped.reshape(GROUPS, group_rows, width), meta, gate_weight[0], up_weight[0],
        down_weight[0], plane, capacity,
    )
    expert_mix = jnp.dot(
        chooser, returned.reshape(-1, width), preferred_element_type=jnp.float32
    )
    return (middle.astype(jnp.float32) + expert_mix).astype(jnp.bfloat16)


def solution(mesh):
    in_specs = (
        P(("sp", "tp"), None),
        P("sp", "tp"),
        P("sp", None),
        P("sp", None),
        P("sp"),
        P(None, "tp"),
        P(None, "tp"),
        P(),
        P(),
        P(),
        P(("sp", "tp"), None),
        P(("sp", "tp"), None),
        P("sp", None, "tp"),
        P("sp", None, "tp"),
        P("sp", "tp", None),
    )
    out_specs = P(("sp", "tp"), None)
    return jax.shard_map(local, mesh=mesh, in_specs=in_specs, out_specs=out_specs, check_vma=False)
```

profile of v0, /device:TPU:0, one launch (start us, length us, event | category | flops | bytes accessed | tf_op | source)
XLA Modules:
  0.0 127.7 jit_solution(5083752167820040190)
XLA Ops:
  0.0 0.7 convert_element_type.50
  0.7 0.8 subtract_convert_fusion
  1.5 0.7 add_bitcast_fusion
  2.2 0.7 fusion.4
  2.9 0.2 select_reduce_fusion.1
  3.1 0.7 select_reduce_fusion
  3.8 0.7 add_convert_fusion
  4.5 0.7 bitcast_add_fusion.1.member_ref
  5.2 0.2 fusion.1
  5.4 0.1 reshape.111
  5.5 0.1 multiply_sine_fusion
  5.7 0.0 copy-start
  5.7 1.9 %copy-done = bf16[768,2048]{1,0:T(8,128)(2,1)S(1)} copy-done((bf16[768,2048]{1,0:T(8,128)(2,1)S(1)}, bf16[768,2048]{1,0:T(8,128)(2,1)}, u32[]{:S(2)}) %copy-start) | copy-done | bytes 3145752
  7.6 0.0 copy-start.2
  7.6 1.0 copy-done.2
  8.6 0.0 copy-start.3
  8.6 1.0 copy-done.3
  9.6 0.0 copy-start.4
  9.6 0.9 copy-done.4
  10.5 0.0 copy-start.5
  10.5 0.9 copy-done.5
  11.4 0.0 copy-start.6
  11.4 0.9 copy-done.6
  12.3 0.0 copy-start.7
  12.3 0.7 copy-done.7
  13.0 0.0 copy-start.8
  13.0 0.7 copy-done.8
  13.7 0.0 copy-start.9
  13.7 0.7 copy-done.9
  14.4 0.0 copy-start.1
  14.4 13.0 %attend.1 = (bf16[128,2048]{1,0:T(8,128)(2,1)S(1)}, bf16[256,2048]{1,0:T(8,128)(2,1)S(1)}) custom-call(bf16[576,256]{1,0:T(8,128)(2,1)S(1)} %bitcast.37, bf16[256,256]{1,0:T(8,128)(2,1)S(1)} %copy-done.6, bf16[32,256]{1,0:T(8,128)(2,1)S(1)} %bitcast.38, bf16[256,384]{1,0:T(8,128)(2,1)S(1)} %copy-done.4, bf16[256,384]{1,0:T(8,128)(2,1)S(1)} %copy-done.5, ...), custom_call_target="tpu_custom_call" | custom-call | tf_op jit(solution)/shard_map/attend/pallas_call | solution.py:563
  27.5 0.0 copy-done.1
  27.5 99.1 %run_experts.1 = bf16[4,64,2048]{2,1,0:T(8,128)(2,1)S(1)} custom-call(bf16[4,64,2048]{2,1,0:T(8,128)(2,1)S(1)} %bitcast.36, bf16[4,16,128]{2,1,0:T(8,128)(2,1)S(1)} %pad.9.meta_ref, bf16[2048,512]{1,0:T(8,128)(2,1)S(1)} %bitcast.35, bf16[2048,512]{1,0:T(8,128)(2,1)} %bitcast.42, bf16[512,2048]{1,0:T(8,128)(2,1)} %bitcast.43), custom_call_target="tpu_custom_call" | custom-call | tf_op jit(solution)/shard_map/run_experts/pallas_call | solution.py:269
  126.6 1.1 fusion
  (8 shorter events, 0.1 us)
Async XLA Ops:
  5.7 1.9 %copy-start = (bf16[768,2048]{1,0:T(8,128)(2,1)S(1)}, bf16[768,2048]{1,0:T(8,128)(2,1)}, u32[]{:S(2)}) copy-start(bf16[768,2048]{1,0:T(8,128)(2,1)} %proj_hbm.1) | copy-start | bytes 9437188
  7.6 1.0 copy-start.2
  8.6 1.0 copy-start.3
  9.6 0.9 copy-start.4
  10.5 0.9 copy-start.5
  11.4 0.9 copy-start.6
  12.3 0.7 copy-start.7
  13.0 0.7 copy-start.8
  13.7 0.7 copy-start.9
  14.4 13.0 %copy-start.1 = (bf16[1,2048,512]{2,1,0:T(8,128)(2,1)S(1)}, bf16[1,2048,512]{2,1,0:T(8,128)(2,1)}, u32[]{:S(2)}) copy-start(bf16[1,2048,512]{2,1,0:T(8,128)(2,1)} %param.27) | copy-start | bytes 6291460
where the time goes:
time: 128 us
  Pallas kernels  112 us (88%)
  local copies, waits for them, and re-layouts  8.91 us (7%)
  other arithmetic  5.11 us (4%)
  matrix products  1.51 us (1%)
    pallas_call x1, Pallas kernels, run_experts(): pl.pallas_call(functools.partial(expert_kernel, groups, plane, capacity),...  99.1 us
    pallas_call x1, Pallas kernels, attend(): pl.pallas_call(functools.partial(attend_kernel, GROUPS, plane, heads), ou...  13 us
    unnamed x20, local copies, waits for them, and re-layouts  8.76 us

commit v1 on v0

v1 whole, which is shorter than its diff:
```python
import functools
import math

import jax
import jax.numpy as jnp
from jax import lax
from jax.experimental import pallas as pl
from jax.experimental.pallas import tpu as pltpu
from jax.sharding import PartitionSpec as P

UNROTATED_DIM = 64
ROPE = 32
VALUE_ENTRIES = 64
GROUPS = 4
HEAD_LANES = 128
VMEM_GRANT = 56 * 1024 * 1024
PARTS = 2
OUTER = "out1 over0 ffn0 over1"
OUTER_MORE = ["back0 ffn1 out2 out3", "over2 ffn2 back2 over3", "ffn3 back3 back1 comb2", "comb3 comb1 comb0"]
INNER = "out1 out2 over0 ffn0"
INNER_MORE = ["over1 ffn1 back1 out3", "over2 ffn2 back2 comb1", "over3 ffn3 back3 back0", "comb2 comb3 comb0"]
MESH = pl.DeviceIdType.MESH

rope_base = 10000.0
epsilon = 1e-06


def angles_of(positions):
    half_width = ROPE // 2
    frequency = rope_base ** (-jnp.arange(half_width, dtype=jnp.float32) / half_width)
    angles = frequency[:, None] * positions.astype(jnp.float32)[None, :]
    return jnp.cos(angles), jnp.sin(angles)


def rms_scale(source, gain):
    return source * lax.rsqrt(jnp.mean(source * source, axis=-1, keepdims=True) + epsilon) * gain


def turn(pair, cosine, sine):
    half = ROPE // 2
    upper, lower = pair[:half].astype(jnp.float32), pair[half:].astype(jnp.float32)
    return jnp.concatenate(
        [upper * cosine - lower * sine, lower * cosine + upper * sine], axis=0
    ).astype(jnp.bfloat16)


def greet(groups, plane, meanwhile=None):
    index, core = lax.axis_index("sp"), lax.axis_index("tp")
    level, place = index // plane, lax.rem(index, plane)
    barrier = pltpu.get_barrier_semaphore()
    peers = [(lax.rem(level + d, groups) * plane + place, core) for d in range(1, groups)]
    peers += [(level * plane + lax.rem(place + d, plane), core) for d in range(1, plane)]
    peers += [(index, 1 - core)]
    for peer in peers:
        pl.semaphore_signal(barrier, inc=1, device_id=peer, device_id_type=MESH)
    if meanwhile is not None:
        meanwhile(index, core)
    pl.semaphore_wait(barrier, len(peers))
    return index, core, level, place


def remote(source, target, send_sem, recv_sem, peer):
    return pltpu.make_async_remote_copy(
        src_ref=source, dst_ref=target, send_sem=send_sem, recv_sem=recv_sem,
        device_id=peer, device_id_type=MESH,
    )


def level_order(groups):
    return sorted(range(groups), key=lambda d: min(d, groups - d))


def nearest(level, groups, at):
    picked = 0
    for l in range(groups):
        choice = sorted(range(groups), key=lambda s: (abs(s - l), s))[at]
        picked = picked + jnp.where(level == l, choice, 0)
    return picked


def expert_stage(
    groups, plane, where, ready, grouped, metas, out_ref,
    gate, up, down, landed, spread, arrived, hidden, partial, passed, mixed, back, merged,
    m_send, m_recv, z_send, z_recv, p_send, p_recv, own_sem, t_send, t_recv,
    x_send, x_recv, b_send, b_recv, keep_sem, r_send, r_recv,
):
    index, core, level, place = where
    started = []
    group_rows, width = grouped.shape[1:]
    capacity = spread.shape[2]
    slots = plane * capacity
    cut = width // PARTS
    source_of = [nearest(level, groups, k) for k in range(groups)]

    def begin(copy):
        copy.start()
        started.append(copy)

    def z_copy(k):
        other = source_of[k]
        return remote(
            grouped.at[other], landed.at[level], z_send.at[k], z_recv.at[level],
            (other * plane + place, core),
        )

    def out_copies(k):
        copies = []
        for far in range(plane - 1, 0, -1):
            to = lax.rem(place + far, plane)
            copies.append(remote(
                spread.at[k, to], arrived.at[k, core, place],
                p_send.at[k * plane + far], p_recv.at[k * plane + place],
                (level * plane + to, core),
            ))
        return copies

    def own_copy(k):
        return pltpu.make_async_copy(
            spread.at[k, place], arrived.at[k, core, place], own_sem.at[k]
        )

    def send_out(k):
        source = source_of[k]
        if k == 0:
            rows = grouped[level]
        else:
            peer = (source * plane + place, core)
            remote(metas.at[source], metas.at[source], m_send.at[k], m_recv.at[source], peer).wait_recv()
            remote(grouped.at[source], landed.at[source], z_send.at[k], z_recv.at[source], peer).wait_recv()
            rows = landed[source]
        info = metas[source][:, :group_rows].astype(jnp.float32)
        slot = lax.broadcasted_iota(jnp.int32, (slots, group_rows), 0).astype(jnp.float32)
        chooser = jnp.where((slot == info[0:1]) | (slot == info[1:2]), 1.0, 0.0)
        picked = jnp.dot(chooser.astype(jnp.bfloat16), rows, preferred_element_type=jnp.float32)
        for e in range(plane):
            spread[k, e] = picked[e * capacity : (e + 1) * capacity].astype(jnp.bfloat16)
        for copy in out_copies(k):
            copy.start()
        own_copy(k).start()

    def hand_over(k):
        for far in range(plane):
            origin = lax.rem(place + plane - far, plane)
            if far:
                remote(
                    spread.at[k, origin], arrived.at[k, core, origin],
                    p_send.at[k * plane + far], p_recv.at[k * plane + origin],
                    (level * plane + origin, core),
                ).wait_recv()
            else:
                own_copy(k).wait()
            begin(remote(
                arrived.at[k, core, origin], arrived.at[k, core, origin],
                t_send.at[k * plane + far], t_recv.at[k * plane + origin], (index, 1 - core),
            ))

    def experts(k):
        for origin in range(plane):
            remote(
                arrived.at[k, 1 - core, origin], arrived.at[k, 1 - core, origin],
                t_send.at[k * plane], t_recv.at[k * plane + origin], (index, 1 - core),
            ).wait_recv()
        units = gate.shape[1]
        unit_tile = math.gcd(units, 256)
        tile = math.gcd(cut, 256)

        def hide(j, carry):
            columns = pl.ds(pl.multiple_of(j * unit_tile, unit_tile), unit_tile)
            rows = arrived[k].reshape(2 * slots, width)
            gated = jnp.dot(rows, gate[:, columns], preferred_element_type=jnp.float32)
            raised = jnp.dot(rows, up[:, columns], preferred_element_type=jnp.float32)
            hidden[:, columns] = (gated / (1.0 + jnp.exp(-gated)) * raised).astype(jnp.bfloat16)
            return carry

        with jax.named_scope(f"E_hide{k}"):
            lax.fori_loop(0, units // unit_tile, hide, 0)
        for part in range(PARTS):

            def lower(j, carry, part=part):
                offset = pl.multiple_of(j * tile, tile)
                columns = pl.ds(pl.multiple_of(part * cut + offset, tile), tile)
                piece = jnp.dot(hidden[...], down[:, columns], preferred_element_type=jnp.float32)
                partial[k, part, :, :, :, pl.ds(offset, tile)] = piece.reshape(
                    2, plane, capacity, tile
                ).astype(jnp.bfloat16)
                return carry

            with jax.named_scope(f"E_lower{k}"):
                lax.fori_loop(0, cut // tile, lower, 0)
            at = k * PARTS + part
            begin(remote(
                partial.at[k, part, 1 - core], passed.at[k, part], x_send.at[at], x_recv.at[at],
                (index, 1 - core),
            ))

    def keep_copy(k, part):
        return pltpu.make_async_copy(
            mixed.at[k, part, place], back.at[k, part, place], keep_sem.at[k * PARTS + part]
        )

    def send_back(k):
        for part in range(PARTS):
            at = k * PARTS + part
            remote(
                partial.at[k, part, core], passed.at[k, part], x_send.at[at], x_recv.at[at],
                (index, 1 - core),
            ).wait_recv()
            for e in range(plane):
                mixed[k, part, e] = (
                    partial[k, part, core, e].astype(jnp.float32) + passed[k, part, e].astype(jnp.float32)
                ).astype(jnp.bfloat16)
            for far in range(plane - 1, 0, -1):
                to = lax.rem(place + far, plane)
                begin(remote(
                    mixed.at[k, part, to], back.at[k, part, place],
                    b_send.at[at * plane + far], b_recv.at[at * plane + place],
                    (level * plane + to, core),
                ))
            keep_copy(k, part).start()

    def combine(k):
        source = source_of[k]
        info = metas[source][:, :group_rows].astype(jnp.float32)
        slot = lax.broadcasted_iota(jnp.int32, (slots, group_rows), 0).astype(jnp.float32)
        hit_first, hit_second = slot == info[0:1], slot == info[1:2]
        for part in range(PARTS):
            at = k * PARTS + part
            for far in range(1, plane):
                origin = lax.rem(place + plane - far, plane)
                remote(
                    mixed.at[k, part, origin], back.at[k, part, origin],
                    b_send.at[at * plane + far], b_recv.at[at * plane + origin],
                    (level * plane + origin, core),
                ).wait_recv()
            keep_copy(k, part).wait()
            returned = back[k, part].reshape(slots, cut)
            result = 0.0
            for term in range(2):
                share = jnp.where(hit_first, info[2 + term : 3 + term], 0.0) + jnp.where(
                    hit_second, info[4 + term : 5 + term], 0.0
                )
                result = result + lax.dot_general(
                    share.astype(jnp.bfloat16), returned, (((0,), (0,)), ((), ())),
                    preferred_element_type=jnp.float32,
                )
            columns = slice(part * cut, (part + 1) * cut)
            if k == 0:
                out_ref[level, :, columns] = result.astype(jnp.bfloat16)
            else:
                merged[k, part] = result.astype(jnp.bfloat16)
                begin(remote(
                    merged.at[k, part], out_ref.at[level, :, columns],
                    r_send.at[at], r_recv.at[level * PARTS + part], (source * plane + place, core),
                ))

    steps = dict(out=send_out, over=hand_over, ffn=experts, back=send_back, comb=combine)

    def staged(name):
        with jax.named_scope("E_" + name):
            steps[name[:-1]](int(name[-1]))

    def finish(order):
        for name in " ".join(order).split():
            staged(name)
        with jax.named_scope("E_rest"):
            for k in range(1, groups):
                other = source_of[k]
                for part in range(PARTS):
                    at = k * PARTS + part
                    remote(
                        merged.at[k, part], out_ref.at[other, :, part * cut : (part + 1) * cut],
                        r_send.at[at], r_recv.at[other * PARTS + part], (other * plane + place, core),
                    ).wait_recv()
        for copy in started:
            copy.wait_send()
        started.clear()

    for k in (1, 0, 2, 3):
        ready(source_of[k])
        if k:
            z_copy(k).start()
        else:
            staged("out0")
    inner = (level > 0) & (level < groups - 1)
    pl.when(inner)(lambda: finish([INNER] + INNER_MORE))
    pl.when(jnp.logical_not(inner))(lambda: finish([OUTER] + OUTER_MORE))
    for k in range(groups):
        if k:
            z_copy(k).wait_send()
        for copy in out_copies(k):
            copy.wait_send()


def assign(groups, plane, expert_ids, route, meta_ref):
    row_count = expert_ids.shape[1]
    count = groups * plane
    capacity = row_count // plane
    group_rows = row_count // 2
    ids = expert_ids.astype(jnp.float32)
    first, second = ids[0:1], ids[1:2]
    bins = -(-(count + groups) // 16) * 16
    line = lax.broadcasted_iota(jnp.int32, (bins, row_count), 0).astype(jnp.float32)
    group = jnp.zeros_like(first)
    for g in range(1, groups):
        group = group + jnp.where(first >= g * plane, 1.0, 0.0)
    hit_first, hit_second = line == first, line == second
    hit_group = line == group + count
    named = jnp.where(hit_first | hit_second | hit_group, 1.0, 0.0).astype(jnp.bfloat16)
    square = (row_count, row_count)
    before = jnp.where(
        lax.broadcasted_iota(jnp.int32, square, 0) < lax.broadcasted_iota(jnp.int32, square, 1), 1.0, 0.0
    ).astype(jnp.bfloat16)
    earlier = jnp.dot(named, before, preferred_element_type=jnp.float32)

    def rank_of(hit):
        return jnp.sum(jnp.where(hit, earlier, 0.0), axis=0, keepdims=True)

    member = group * group_rows + rank_of(hit_group)
    base = group * plane
    fields = [
        (first - base) * capacity + rank_of(hit_first) + 1.0,
        (second - base) * capacity + rank_of(hit_second) + 1.0,
    ]
    for term in range(2):
        weight = route[term : term + 1]
        coarse = weight.astype(jnp.bfloat16).astype(jnp.float32)
        fields += [coarse, weight - coarse]
    line = lax.broadcasted_iota(jnp.int32, (16, row_count), 0)
    table = jnp.zeros((16, row_count), jnp.float32)
    for at, field in enumerate(fields):
        table = jnp.where(line == at, field, table)
    table = table.astype(jnp.bfloat16)
    lanes = meta_ref.shape[2]
    spot = lax.broadcasted_iota(jnp.int32, (lanes, row_count), 0).astype(jnp.float32)
    free = jnp.where(lax.broadcasted_iota(jnp.int32, (16, lanes), 0) < 2, 1.0, 0.0)
    for g in range(groups):
        taken = (spot + g * group_rows == member) & (spot < group_rows)
        info = lax.dot_general(
            table, jnp.where(taken, 1.0, 0.0).astype(jnp.bfloat16), (((1,), (1,)), ((), ())),
            preferred_element_type=jnp.float32,
        )
        meta_ref[g] = (info - free).astype(jnp.bfloat16)
    return member


def layer_kernel(
    groups, plane, heads,
    query_hbm, latent_hbm, rope_hbm, wk_hbm, wv_hbm, proj_hbm, residual_hbm,
    ids_hbm, docs_hbm, route_hbm, mix_gain_hbm, moe_gain_hbm, gate_hbm, up_hbm, down_hbm,
    cos_ref, sin_ref, middle_ref, chooser_ref, out_ref,
    query, latent, rope, wk, wv, proj, residual, expert_ids, doc_ids, route, mix_gain, moe_gain,
    gate, up, down,
    packs, turned, wv_turned, high, total, acc, halves, full, mix, normed, grouped, meta, metas,
    load_sem, z_send, z_recv, p_send, p_recv, t_send, t_recv, x_send, x_recv, m_send, m_recv, *rest,
):
    loads = [
        pltpu.make_async_copy(source, target, load_sem.at[i])
        for i, (source, target) in enumerate([
            (latent_hbm, latent), (rope_hbm, rope), (docs_hbm, doc_ids), (query_hbm, query),
            (wk_hbm, wk), (wv_hbm, wv), (ids_hbm, expert_ids), (route_hbm, route),
            (mix_gain_hbm, mix_gain), (moe_gain_hbm, moe_gain), (residual_hbm, residual),
            (proj_hbm, proj), (gate_hbm, gate), (up_hbm, up), (down_hbm, down),
        ])
    ]
    for copy in loads:
        copy.start()
    rows = latent.shape[0]
    half = rows // 2
    per_head = UNROTATED_DIM + ROPE
    cosine, sine = cos_ref[...], sin_ref[...]

    def pack(index, core):
        for copy in loads[:3]:
            copy.wait()
        docs = doc_ids[...].astype(jnp.float32)
        key = turn(rope[...], cosine, sine)
        for part in range(2):
            span = slice(part * half, (part + 1) * half)
            packs[index, part, :half, :] = latent[span, :]
            line = lax.broadcasted_iota(jnp.int32, (ROPE, half), 0)
            ids = jnp.where(line == 0, jnp.broadcast_to(docs[:, span], (ROPE, half)), 0.0)
            packs[index, part, half:, :half] = key[:, span]
            packs[index, part, half:, half : 2 * half] = ids.astype(jnp.bfloat16)

    with jax.named_scope("A_greet"):
        index, core, level, place = greet(groups, plane, pack)
    reach = groups // 2

    def z_copy(d):
        return remote(
            packs.at[index, core], packs.at[index, core], z_send.at[d], z_recv.at[d],
            (lax.rem(level + d, groups) * plane + place, core),
        )

    def z_arrival(d):
        block = lax.rem(level + groups - d, groups) * plane + place
        return remote(
            packs.at[block, core], packs.at[block, core], z_send.at[d], z_recv.at[d],
            (block, core),
        )

    def p_copy(d, far):
        block = lax.rem(level + groups - d, groups) * plane + place
        return remote(
            packs.at[block, core], packs.at[block, core], p_send.at[d * plane + far],
            p_recv.at[d * plane + far],
            (level * plane + lax.rem(place + far, plane), core),
        )

    def p_arrival(d, far):
        origin = lax.rem(place + plane - far, plane)
        block = lax.rem(level + groups - d, groups) * plane + origin
        return remote(
            packs.at[block, core], packs.at[block, core], p_send.at[d * plane + far],
            p_recv.at[d * plane + far], (level * plane + origin, core),
        )

    def t_copy(d, far, part):
        origin = lax.rem(place + plane - far, plane)
        block = lax.rem(level + groups - d, groups) * plane + origin
        return remote(
            packs.at[block, part], packs.at[block, part], t_send.at[d * plane + far],
            t_recv.at[d * plane + far], (index, 1 - core),
        )

    def wanted(d, far, sender):
        ahead = lax.rem(place + far, plane) > place if sender else place >= far
        live = level >= d
        if d == 0:
            return live & ahead
        if d == reach:
            return live & jnp.logical_not(ahead)
        return live

    for d in range(1, reach + 1):
        pl.when(level + d < groups)(lambda d=d: z_copy(d).start())
    for far in range(1, plane):
        pl.when(wanted(0, far, True))(lambda far=far: p_copy(0, far).start())

    for copy in loads[3:10]:
        copy.wait()
    docs = doc_ids[...].astype(jnp.float32)
    with jax.named_scope("A_assign"):
        member = assign(groups, plane, expert_ids[...], route[...], meta)
    metas[level] = meta[level]

    def m_copy(k):
        other = nearest(level, groups, k)
        return remote(
            meta.at[other], metas.at[level], m_send.at[k], m_recv.at[level],
            (other * plane + place, core),
        )

    for k in range(1, groups):
        m_copy(k).start()
    blank = jnp.zeros((HEAD_LANES - per_head, rows), jnp.bfloat16)
    for h in range(heads):
        own = query[h * per_head : (h + 1) * per_head, :]
        plain, moved = own[:UNROTATED_DIM], turn(own[UNROTATED_DIM:], cosine, sine)
        parts = [plain, moved, blank] if h % 2 == 0 else [moved, blank, plain]
        turned[h] = jnp.concatenate(parts, axis=0)
    wv_turned[...] = wv[...].astype(jnp.float32).T.astype(jnp.bfloat16)
    power = per_head ** (-0.5) * math.log2(math.e)

    def attend(block, first):
        source = jnp.concatenate([packs[block, part, :half, :] for part in range(2)], axis=0)
        tail = jnp.concatenate(
            [
                jnp.concatenate([packs[block, part, half:, :half] for part in range(2)], axis=1),
                jnp.concatenate(
                    [packs[block, part, half : half + 16, half : 2 * half] for part in range(2)], axis=1
                ),
            ],
            axis=0,
        )
        shape = (ROPE + 16, 3 * HEAD_LANES)
        line = lax.broadcasted_iota(jnp.int32, shape, 0)
        lane = lax.broadcasted_iota(jnp.int32, shape, 1)
        keyed = (line < ROPE) & ((lane == line + UNROTATED_DIM) | (lane == line + 2 * HEAD_LANES))
        named = (line == ROPE) & (lane >= HEAD_LANES) & (lane < 2 * HEAD_LANES)
        chooser = jnp.where(keyed | named, 1.0, 0.0).astype(jnp.bfloat16)
        extra = lax.dot_general(
            tail, chooser, (((0,), (0,)), ((), ())), preferred_element_type=jnp.float32
        )
        extras = [
            extra[:, :HEAD_LANES].astype(jnp.bfloat16), extra[:, 2 * HEAD_LANES :].astype(jnp.bfloat16)
        ]
        theirs = extra[:, HEAD_LANES : 2 * HEAD_LANES]
        theirs = jnp.concatenate([theirs] * (rows // HEAD_LANES), axis=1)
        live = theirs == docs
        if first:
            live = live & (
                lax.broadcasted_iota(jnp.int32, (rows, rows), 0)
                <= lax.broadcasted_iota(jnp.int32, (rows, rows), 1)
            )
        bias = jnp.where(live, 0.0, -1e30)
        keys = jnp.dot(source, wk[...], preferred_element_type=jnp.float32).astype(jnp.bfloat16)
        values = lax.dot_general(
            wv_turned[...], source, (((1,), (1,)), ((), ())), preferred_element_type=jnp.float32
        ).astype(jnp.bfloat16)
        side = lax.broadcasted_iota(jnp.int32, (rows, HEAD_LANES), 1) < UNROTATED_DIM
        for h in range(heads):
            low = h // 2 * HEAD_LANES
            pair = keys[:, low : low + HEAD_LANES]
            key = jnp.where(side, pair, extras[0]) if h % 2 == 0 else jnp.where(side, extras[1], pair)
            scores = jnp.dot(key, turned[h], preferred_element_type=jnp.float32) + bias
            top = jnp.max(scores, axis=0, keepdims=True)
            if not first:
                old = high[h : h + 1, :]
                top = jnp.maximum(old, top)
            weights = jnp.exp2((scores - top) * power)
            mass = jnp.sum(weights, axis=0, keepdims=True)
            mixed = jnp.dot(
                values[h * VALUE_ENTRIES : (h + 1) * VALUE_ENTRIES], weights.astype(jnp.bfloat16),
                preferred_element_type=jnp.float32,
            )
            high[h : h + 1, :] = top
            if first:
                total[h : h + 1, :] = mass
                acc[h] = mixed
            else:
                factor = jnp.exp2((old - top) * power)
                total[h : h + 1, :] = total[h : h + 1, :] * factor + mass
                acc[h] = acc[h] * factor + mixed

    with jax.named_scope("A_own"):
        attend(index, True)

    def relay(d):
        def arrived():
            with jax.named_scope(f"A_z{d}"):
                z_arrival(d).wait_recv()
            t_copy(d, 0, core).start()

        pl.when(level >= d)(arrived)
        for far in range(1, plane):
            pl.when(wanted(d, far, True))(lambda: p_copy(d, far).start())

    relay(1)

    def where_is(t):
        block = index - t
        d = level - block // plane
        far = lax.rem(place + plane - lax.rem(block, plane), plane)
        return block, d, far

    def pass_on(t):
        block, d, far = where_is(t)

        def passed():
            with jax.named_scope("A_pass"):
                p_arrival(d, far).wait_recv()
            t_copy(d, far, core).start()

        pl.when(far > 0)(passed)

    last = jnp.minimum(index, reach * plane)
    pl.when(last > 0)(lambda: pass_on(1))

    def step(t, carry):
        @pl.when(t == place + 1)
        def _():
            for d in range(2, reach + 1):
                relay(d)

        pl.when(t < last)(lambda: pass_on(t + 1))
        block, d, far = where_is(t)
        with jax.named_scope("A_wait"):
            t_copy(d, far, 1 - core).wait_recv()
        with jax.named_scope("A_block"):
            attend(block, False)
        return carry

    lax.fori_loop(1, last + 1, step, 0)

    for h in range(heads):
        done = (acc[h] / total[h : h + 1, :]).astype(jnp.bfloat16)
        for part in range(2):
            halves[part, h * VALUE_ENTRIES : (h + 1) * VALUE_ENTRIES, :] = done[:, part * half : (part + 1) * half]
    swap = remote(halves.at[1 - core], full.at[core], x_send, x_recv, (index, 1 - core))
    swap.start()
    full[core] = halves[core]
    loads[10].wait()
    loads[11].wait()
    with jax.named_scope("A_swap"):
        remote(halves.at[core], full.at[1 - core], x_send, x_recv, (index, 1 - core)).wait_recv()
    width = proj.shape[1]
    tile = math.gcd(width, 512)
    attended = full[...].reshape(proj.shape[0], half).astype(jnp.float32).T.astype(jnp.bfloat16)

    def project(j, carry):
        columns = pl.ds(pl.multiple_of(j * tile, tile), tile)
        mix[:, columns] = jnp.dot(attended, proj[:, columns], preferred_element_type=jnp.float32)
        return carry

    with jax.named_scope("A_project"):
        lax.fori_loop(0, width // tile, project, 0)

    def settle(j, carry):
        some = pl.ds(pl.multiple_of(j * 16, 16), 16)
        branch = rms_scale(mix[some, :], mix_gain[...])
        middle = (residual[some, :].astype(jnp.float32) + branch).astype(jnp.bfloat16)
        middle_ref[some, :] = middle
        normed[some, :] = rms_scale(middle.astype(jnp.float32), moe_gain[...]).astype(jnp.bfloat16)
        return carry

    with jax.named_scope("A_settle"):
        lax.fori_loop(0, half // 16, settle, 0, unroll=2)
    group_rows = grouped.shape[1]
    slots = groups * group_rows
    chooser_ref[...] = jnp.where(
        lax.broadcasted_iota(jnp.int32, (slots, half), 0).astype(jnp.float32) == member, 1.0, 0.0
    ).astype(jnp.bfloat16)

    def ready(group):
        picks = chooser_ref[pl.ds(pl.multiple_of(group * group_rows, group_rows), group_rows), :]
        for j in range(width // tile):
            columns = slice(j * tile, (j + 1) * tile)
            grouped[group, :, columns] = jnp.dot(
                picks, normed[:, columns], preferred_element_type=jnp.float32
            ).astype(jnp.bfloat16)

    for copy in loads[12:]:
        copy.wait()
    expert_stage(
        groups, plane, (index, core, level, place), ready, grouped, metas, out_ref,
        gate, up, down, *rest[:9], m_send, m_recv, *rest[9:],
    )

    swap.wait_send()
    for d in range(reach + 1):
        for far in range(0 if d else 1, plane):
            pl.when((level >= d) if far == 0 else wanted(d, far, False))(
                lambda d=d, far=far: t_copy(d, far, core).wait_send()
            )
            if far:
                pl.when(wanted(d, far, True))(lambda d=d, far=far: p_copy(d, far).wait_send())
    for d in range(1, reach + 1):
        pl.when(level + d < groups)(lambda d=d: z_copy(d).wait_send())
    for k in range(1, groups):
        m_copy(k).wait_send()


def layer(
    queries, latent, rope_key, wk, wv, proj, residual, expert_ids, doc_ids, route,
    mix_gain, moe_gain, gate, up, down, cosine, sine, count,
):
    rows, rank = latent.shape
    half = rows // 2
    plane = count // GROUPS
    capacity = half // plane
    heads = wk.shape[1] // UNROTATED_DIM
    width = proj.shape[1]
    units = gate.shape[1]
    group_rows = half // 2
    cut = width // PARTS
    vmem = pl.BlockSpec(memory_space=pltpu.VMEM)
    hbm = pl.BlockSpec(memory_space=pltpu.HBM)
    dma = pltpu.SemaphoreType.DMA
    few, many = dma((GROUPS,)), dma((GROUPS * plane,))
    few_parts, many_parts = dma((GROUPS * PARTS,)), dma((GROUPS * PARTS * plane,))

    def held(*shape, dtype=jnp.bfloat16):
        return pltpu.VMEM(shape, dtype)

    loaded = (
        queries.T, latent, rope_key.T, wk, wv, proj, residual, expert_ids.T, doc_ids[None, :],
        route.T, mix_gain[None, :], moe_gain[None, :], gate, up, down,
    )
    table = held(GROUPS, 16, -(-group_rows // 128) * 128)
    block = held(GROUPS, PARTS, plane, capacity, cut)
    return pl.pallas_call(
        functools.partial(layer_kernel, GROUPS, plane, heads),
        out_shape=(
            jax.ShapeDtypeStruct((half, width), jnp.bfloat16),
            jax.ShapeDtypeStruct((GROUPS * group_rows, half), jnp.bfloat16),
            jax.ShapeDtypeStruct((GROUPS, group_rows, width), jnp.bfloat16),
        ),
        in_specs=[hbm] * len(loaded) + [vmem] * 2,
        out_specs=(vmem,) * 3,
        scratch_shapes=[held(*array.shape, dtype=array.dtype) for array in loaded] + [
            held(count, 2, half + ROPE, rank),
            held(heads, HEAD_LANES, rows),
            held(heads * VALUE_ENTRIES, rank),
            held(heads, rows, dtype=jnp.float32),
            held(heads, rows, dtype=jnp.float32),
            held(heads, VALUE_ENTRIES, rows, dtype=jnp.float32),
            held(2, heads * VALUE_ENTRIES, half),
            held(2, heads * VALUE_ENTRIES, half),
            held(half, width, dtype=jnp.float32),
            held(half, width),
            held(GROUPS, group_rows, width), table, table,
            dma((len(loaded),)), few, few, many, many, many, many, dma, dma, few, few,
            held(GROUPS, group_rows, width),
            held(GROUPS, plane, capacity, width),
            held(GROUPS, 2, plane, capacity, width),
            held(2 * plane * capacity, units),
            held(GROUPS, PARTS, 2, plane, capacity, cut),
            block, block, block,
            held(GROUPS, PARTS, group_rows, cut),
            few, few, many, many, few, many, many,
            few_parts, few_parts, many_parts, many_parts, few_parts, few_parts, few_parts,
        ],
        compiler_params=pltpu.CompilerParams(
            collective_id=3, has_side_effects=True, vmem_limit_bytes=VMEM_GRANT
        ),
        name="layer",
    )(*loaded, cosine, sine)


def local(
    residual,
    queries,
    latent,
    rope_key,
    doc_ids,
    latent_to_key,
    latent_to_value,
    out_proj,
    mix_gain,
    moe_gain,
    expert_ids,
    route_weight,
    gate_weight,
    up_weight,
    down_weight,
):
    local_rows = queries.shape[0]
    positions = lax.axis_index("sp") * local_rows + jnp.arange(local_rows, dtype=jnp.int32)
    cosine, sine = angles_of(positions)
    middle, chooser, returned = layer(
        queries, latent, rope_key, latent_to_key, latent_to_value, out_proj, residual,
        expert_ids, doc_ids, route_weight, mix_gain, moe_gain, gate_weight[0], up_weight[0],
        down_weight[0], cosine, sine, lax.axis_size("sp"),
    )
    expert_mix = lax.dot_general(
        chooser, returned.reshape(chooser.shape[0], -1), (((0,), (0,)), ((), ())),
        preferred_element_type=jnp.float32,
    )
    return (middle.astype(jnp.float32) + expert_mix).astype(jnp.bfloat16)


def solution(mesh):
    in_specs = (
        P(("sp", "tp"), None),
        P("sp", "tp"),
        P("sp", None),
        P("sp", None),
        P("sp"),
        P(None, "tp"),
        P(None, "tp"),
        P(),
        P(),
        P(),
        P(("sp", "tp"), None),
        P(("sp", "tp"), None),
        P("sp", None, "tp"),
        P("sp", None, "tp"),
        P("sp", "tp", None),
    )
    out_specs = P(("sp", "tp"), None)
    return jax.shard_map(local, mesh=mesh, in_specs=in_specs, out_specs=out_specs, check_vma=False)
```

time: 128 us -> 110 us (0.86)
  local copies, waits for them, and re-layouts: 8.91 us -> 0 us
  Pallas kernels: 112 us -> 105 us
  other arithmetic: 5.11 us -> 0.77 us
    unnamed x20 -> x0, local copies, waits for them, and re-layouts: 8.76 us -> none
    pallas_call x2 -> x1, Pallas kernels: 112 us -> 105 us  [layer(): pl.pallas_call(functools.partial(layer_kernel, GROUPS, plane, heads), out...]
    convert_element_type x4 -> x0, other arithmetic: 2.13 us -> none  [the longest x1 0.76 us: local(): fine = (route_weight - coarse.astype(jnp.float32)).astype(jnp.bfloat16)]
where the time goes in v1:
time: 110 us; the launch traced here: 109 us
  Pallas kernels  105 us (95%)
  matrix products  2.51 us (2%)
    pallas_call x1, Pallas kernels, layer(): pl.pallas_call(functools.partial(layer_kernel, GROUPS, plane, heads), out...  105 us
    dot_general x1, matrix products, local(): lax.dot_general(chooser, returned.reshape(chooser.shape[0], -1), (((0,),...  2.51 us

profile of v1, /device:TPU:0, one launch (start us, length us, event | category | flops | bytes accessed | tf_op | source)
XLA Modules:
  0.0 108.7 jit_solution(11030243455135896249)
XLA Ops:
  0.0 0.8 multiply_sine_fusion
  0.8 105.4 %layer.1 = (bf16[128,2048]{1,0:T(8,128)(2,1)}, bf16[256,128]{1,0:T(8,128)(2,1)}, bf16[4,64,2048]{2,1,0:T(8,128)(2,1)}) custom-call(bf16[576,256]{1,0:T(8,128)(2,1)} %bitcast.17, bf16[256,256]{1,0:T(8,128)(2,1)} %latent_hbm.1, bf16[32,256]{1,0:T(8,128)(2,1)} %bitcast.18, bf16[256,384]{1,0:T(8,128)(2,1)} %wk_hbm.1, bf16[256,384]{1,0:T(8,128)(2,1)} %wv_hbm.1, ...), custom_call_target="tpu_custom_call" | custom-call | tf_op jit(solution)/shard_map/layer/pallas_call | solution.py:672
  106.1 2.5 %fusion = bf16[128,2048]{1,0:T(8,128)(2,1)} fusion(bf16[256,128]{1,0:T(8,128)(2,1)} %get-tuple-element.9, bf16[256,2048]{1,0:T(8,128)(2,1)} %bitcast.16, bf16[128,2048]{1,0:T(8,128)(2,1)} %get-tuple-element.8), kind=kOutput, calls=%fused_computation.1 | convolution fusion | flops 135004160 | bytes 2162688 | tf_op jit(solution)/shard_map/dot_general | solution.py:736
  (2 shorter events, 0.0 us)

commit v2 on v1

--- a/solution.py
+++ b/solution.py
@@ -25,10 +25,14 @@
 epsilon = 1e-06
 
 
-def angles_of(positions):
+def angles_of(first, count):
     half_width = ROPE // 2
-    frequency = rope_base ** (-jnp.arange(half_width, dtype=jnp.float32) / half_width)
-    angles = frequency[:, None] * positions.astype(jnp.float32)[None, :]
+    line = lax.broadcasted_iota(jnp.int32, (half_width, count), 0)
+    frequency = jnp.zeros((half_width, count), jnp.float32)
+    for i in range(half_width):
+        frequency = jnp.where(line == i, rope_base ** (-i / half_width), frequency)
+    positions = first + lax.broadcasted_iota(jnp.int32, (half_width, count), 1)
+    angles = positions.astype(jnp.float32) * frequency
     return jnp.cos(angles), jnp.sin(angles)
 
 
@@ -73,8 +77,10 @@
 def nearest(level, groups, at):
     picked = 0
     for l in range(groups):
-        choice = sorted(range(groups), key=lambda s: (abs(s - l), s))[at]
-        picked = picked + jnp.where(level == l, choice, 0)
+        order = sorted(range(groups), key=lambda s: (abs(s - l), s))
+        if l in (0, groups - 1):
+            order[2:] = order[:1:-1]
+        picked = picked + jnp.where(level == l, order[at], 0)
     return picked
 
 
@@ -347,9 +353,9 @@
     groups, plane, heads,
     query_hbm, latent_hbm, rope_hbm, wk_hbm, wv_hbm, proj_hbm, residual_hbm,
     ids_hbm, docs_hbm, route_hbm, mix_gain_hbm, moe_gain_hbm, gate_hbm, up_hbm, down_hbm,
-    cos_ref, sin_ref, middle_ref, chooser_ref, out_ref,
+    out_ref,
     query, latent, rope, wk, wv, proj, residual, expert_ids, doc_ids, route, mix_gain, moe_gain,
-    gate, up, down,
+    gate, up, down, middle, chooser, returned,
     packs, turned, wv_turned, high, total, acc, halves, full, mix, normed, grouped, meta, metas,
     load_sem, z_send, z_recv, p_send, p_recv, t_send, t_recv, x_send, x_recv, m_send, m_recv, *rest,
 ):
@@ -367,7 +373,7 @@
     rows = latent.shape[0]
     half = rows // 2
     per_head = UNROTATED_DIM + ROPE
-    cosine, sine = cos_ref[...], sin_ref[...]
+    cosine, sine = angles_of(lax.axis_index("sp") * rows, rows)
 
     def pack(index, core):
         for copy in loads[:3]:
@@ -539,9 +545,13 @@
     relay(1)
 
     def where_is(t):
-        block = index - t
-        d = level - block // plane
-        far = lax.rem(place + plane - lax.rem(block, plane), plane)
+        below = t > place
+        turn_at = jnp.where(below, t - place - 1, 0)
+        d = jnp.where(below, 1 + turn_at // plane, 0)
+        far = lax.rem(turn_at, plane)
+        far = jnp.where((d == reach) & (far > 0), place + far, far)
+        far = jnp.where(below, far, t)
+        block = (level - d) * plane + lax.rem(place + plane - far, plane)
         return block, d, far
 
     def pass_on(t):
@@ -558,17 +568,19 @@
     pl.when(last > 0)(lambda: pass_on(1))
 
     def step(t, carry):
-        @pl.when(t == place + 1)
-        def _():
-            for d in range(2, reach + 1):
-                relay(d)
-
-        pl.when(t < last)(lambda: pass_on(t + 1))
+        pl.when((t < last) & (t != place + 1))(lambda: pass_on(t + 1))
         block, d, far = where_is(t)
         with jax.named_scope("A_wait"):
             t_copy(d, far, 1 - core).wait_recv()
         with jax.named_scope("A_block"):
             attend(block, False)
+
+        @pl.when(t == place + 1)
+        def _():
+            for d in range(2, reach + 1):
+                relay(d)
+            pl.when(t < last)(lambda: pass_on(t + 1))
+
         return carry
 
     lax.fori_loop(1, last + 1, step, 0)
@@ -599,21 +611,21 @@
     def settle(j, carry):
         some = pl.ds(pl.multiple_of(j * 16, 16), 16)
         branch = rms_scale(mix[some, :], mix_gain[...])
-        middle = (residual[some, :].astype(jnp.float32) + branch).astype(jnp.bfloat16)
-        middle_ref[some, :] = middle
-        normed[some, :] = rms_scale(middle.astype(jnp.float32), moe_gain[...]).astype(jnp.bfloat16)
+        kept = (residual[some, :].astype(jnp.float32) + branch).astype(jnp.bfloat16)
+        middle[some, :] = kept
+        normed[some, :] = rms_scale(kept.astype(jnp.float32), moe_gain[...]).astype(jnp.bfloat16)
         return carry
 
     with jax.named_scope("A_settle"):
         lax.fori_loop(0, half // 16, settle, 0, unroll=2)
     group_rows = grouped.shape[1]
     slots = groups * group_rows
-    chooser_ref[...] = jnp.where(
+    chooser[...] = jnp.where(
         lax.broadcasted_iota(jnp.int32, (slots, half), 0).astype(jnp.float32) == member, 1.0, 0.0
     ).astype(jnp.bfloat16)
 
     def ready(group):
-        picks = chooser_ref[pl.ds(pl.multiple_of(group * group_rows, group_rows), group_rows), :]
+        picks = chooser[pl.ds(pl.multiple_of(group * group_rows, group_rows), group_rows), :]
         for j in range(width // tile):
             columns = slice(j * tile, (j + 1) * tile)
             grouped[group, :, columns] = jnp.dot(
@@ -623,10 +635,17 @@
     for copy in loads[12:]:
         copy.wait()
     expert_stage(
-        groups, plane, (index, core, level, place), ready, grouped, metas, out_ref,
+        groups, plane, (index, core, level, place), ready, grouped, metas, returned,
         gate, up, down, *rest[:9], m_send, m_recv, *rest[9:],
     )
 
+    spots = chooser[...].astype(jnp.float32).T.astype(jnp.bfloat16)
+    for j in range(width // tile):
+        columns = slice(j * tile, (j + 1) * tile)
+        mixed = jnp.dot(
+            spots, returned[:, :, columns].reshape(slots, tile), preferred_element_type=jnp.float32
+        )
+        out_ref[:, columns] = (middle[:, columns].astype(jnp.float32) + mixed).astype(jnp.bfloat16)
     swap.wait_send()
     for d in range(reach + 1):
         for far in range(0 if d else 1, plane):
@@ -643,7 +662,7 @@
 
 def layer(
     queries, latent, rope_key, wk, wv, proj, residual, expert_ids, doc_ids, route,
-    mix_gain, moe_gain, gate, up, down, cosine, sine, count,
+    mix_gain, moe_gain, gate, up, down, count,
 ):
     rows, rank = latent.shape
     half = rows // 2
@@ -671,14 +690,11 @@
     block = held(GROUPS, PARTS, plane, capacity, cut)
     return pl.pallas_call(
         functools.partial(layer_kernel, GROUPS, plane, heads),
-        out_shape=(
-            jax.ShapeDtypeStruct((half, width), jnp.bfloat16),
-            jax.ShapeDtypeStruct((GROUPS * group_rows, half), jnp.bfloat16),
-            jax.ShapeDtypeStruct((GROUPS, group_rows, width), jnp.bfloat16),
-        ),
-        in_specs=[hbm] * len(loaded) + [vmem] * 2,
-        out_specs=(vmem,) * 3,
+        out_shape=jax.ShapeDtypeStruct((half, width), jnp.bfloat16),
+        in_specs=[hbm] * len(loaded),
+        out_specs=vmem,
         scratch_shapes=[held(*array.shape, dtype=array.dtype) for array in loaded] + [
+            held(half, width), held(GROUPS * group_rows, half), held(GROUPS, group_rows, width),
             held(count, 2, half + ROPE, rank),
             held(heads, HEAD_LANES, rows),
             held(heads * VALUE_ENTRIES, rank),
@@ -705,7 +721,7 @@
             collective_id=3, has_side_effects=True, vmem_limit_bytes=VMEM_GRANT
         ),
         name="layer",
-    )(*loaded, cosine, sine)
+    )(*loaded)
 
 
 def local(
@@ -725,19 +741,11 @@
     up_weight,
     down_weight,
 ):
-    local_rows = queries.shape[0]
-    positions = lax.axis_index("sp") * local_rows + jnp.arange(local_rows, dtype=jnp.int32)
-    cosine, sine = angles_of(positions)
-    middle, chooser, returned = layer(
+    return layer(
         queries, latent, rope_key, latent_to_key, latent_to_value, out_proj, residual,
         expert_ids, doc_ids, route_weight, mix_gain, moe_gain, gate_weight[0], up_weight[0],
-        down_weight[0], cosine, sine, lax.axis_size("sp"),
+        down_weight[0], lax.axis_size("sp"),
     )
-    expert_mix = lax.dot_general(
-        chooser, returned.reshape(chooser.shape[0], -1), (((0,), (0,)), ((), ())),
-        preferred_element_type=jnp.float32,
-    )
-    return (middle.astype(jnp.float32) + expert_mix).astype(jnp.bfloat16)
 
 
 def solution(mesh):

time: 110 us -> 107 us (0.973)
  matrix products: 2.51 us -> 0 us
  local copies, waits for them, and re-layouts: 0 us -> 1.88 us
    dot_general x1 -> x0, matrix products: 2.51 us -> none  [local(): lax.dot_general(chooser, returned.reshape(chooser.shape[0], -1), (((0,),...]
    unnamed x0 -> x1, local copies, waits for them, and re-layouts: none -> 1.88 us
where the time goes in v2:
time: 107 us; the launch traced here: 106 us
  Pallas kernels  105 us (98%)
  local copies, waits for them, and re-layouts  1.88 us (2%)
    pallas_call x1, Pallas kernels, layer(): pl.pallas_call(functools.partial(layer_kernel, GROUPS, plane, heads), out...  105 us

profile of v2, /device:TPU:0, one launch (start us, length us, event | category | flops | bytes accessed | tf_op | source)
XLA Modules:
  0.0 106.4 jit_solution(10997477540551728824)
XLA Ops:
  0.0 104.5 %layer.1 = bf16[128,2048]{1,0:T(8,128)(2,1)} custom-call(bf16[576,256]{1,0:T(8,128)(2,1)} %bitcast.13, bf16[256,256]{1,0:T(8,128)(2,1)} %latent_hbm.1, bf16[32,256]{1,0:T(8,128)(2,1)} %bitcast.14, bf16[256,384]{1,0:T(8,128)(2,1)} %wk_hbm.1, bf16[256,384]{1,0:T(8,128)(2,1)} %wv_hbm.1, bf16[768,2048]{1,0:T(8,128)(2,1)} %proj_hbm.1, ...), custom_call_target="tpu_custom_call" | custom-call | tf_op jit(solution)/shard_map/layer/pallas_call | solution.py:691
  104.5 1.9 %copy.17 = bf16[128,2048]{1,0:T(8,128)(2,1)} copy(bf16[128,2048]{1,0:T(8,128)(2,1)} %layer.1) | data formatting | bytes 1048576

commit v3 on v2

--- a/solution.py
+++ b/solution.py
@@ -15,10 +15,10 @@
 HEAD_LANES = 128
 VMEM_GRANT = 56 * 1024 * 1024
 PARTS = 2
-OUTER = "out1 over0 ffn0 over1"
-OUTER_MORE = ["back0 ffn1 out2 out3", "over2 ffn2 back2 over3", "ffn3 back3 back1 comb2", "comb3 comb1 comb0"]
-INNER = "out1 out2 over0 ffn0"
-INNER_MORE = ["over1 ffn1 back1 out3", "over2 ffn2 back2 comb1", "over3 ffn3 back3 back0", "comb2 comb3 comb0"]
+SOURCES = ((0, 1, 3, 2), (1, 0, 2, 3), (2, 0, 1, 3), (3, 0, 1, 2))
+TARGETS = ((0, 1, 3, 2), (1, 2, 3, 0), (2, 1, 0, 3), (3, 0, 1, 2))
+LOWER = ["out1 over0 ffn0 out2", "over1 ffn1 out3 over2", "ffn2 back2 over3 ffn3", "back3 back1 back0 comb2", "comb3 comb1 comb0"]
+UPPER = ["out1 out2 over0 ffn0", "over1 ffn1 back1 out3", "over2 ffn2 back2 comb1", "over3 ffn3 back3 back0", "comb2 comb3 comb0"]
 MESH = pl.DeviceIdType.MESH
 
 rope_base = 10000.0
@@ -74,12 +74,9 @@
     return sorted(range(groups), key=lambda d: min(d, groups - d))
 
 
-def nearest(level, groups, at):
+def chosen(table, level, at):
     picked = 0
-    for l in range(groups):
-        order = sorted(range(groups), key=lambda s: (abs(s - l), s))
-        if l in (0, groups - 1):
-            order[2:] = order[:1:-1]
+    for l, order in enumerate(table):
         picked = picked + jnp.where(level == l, order[at], 0)
     return picked
 
@@ -96,14 +93,15 @@
     capacity = spread.shape[2]
     slots = plane * capacity
     cut = width // PARTS
-    source_of = [nearest(level, groups, k) for k in range(groups)]
+    source_of = [chosen(SOURCES, level, k) for k in range(groups)]
+    target_of = [chosen(TARGETS, level, k) for k in range(groups)]
 
     def begin(copy):
         copy.start()
         started.append(copy)
 
     def z_copy(k):
-        other = source_of[k]
+        other = target_of[k]
         return remote(
             grouped.at[other], landed.at[level], z_send.at[k], z_recv.at[level],
             (other * plane + place, core),
@@ -282,14 +280,13 @@
         started.clear()
 
     for k in (1, 0, 2, 3):
-        ready(source_of[k])
+        ready(target_of[k])
         if k:
             z_copy(k).start()
         else:
             staged("out0")
-    inner = (level > 0) & (level < groups - 1)
-    pl.when(inner)(lambda: finish([INNER] + INNER_MORE))
-    pl.when(jnp.logical_not(inner))(lambda: finish([OUTER] + OUTER_MORE))
+    pl.when(level < groups // 2)(lambda: finish(LOWER))
+    pl.when(level >= groups // 2)(lambda: finish(UPPER))
     for k in range(groups):
         if k:
             z_copy(k).wait_send()
@@ -429,6 +426,9 @@
             t_recv.at[d * plane + far], (index, 1 - core),
         )
 
+    odd = lax.rem(place, 2) == 1
+    spans = [jnp.where(odd, plane - far, far) for far in range(1, plane)]
+
     def wanted(d, far, sender):
         ahead = lax.rem(place + far, plane) > place if sender else place >= far
         live = level >= d
@@ -440,7 +440,7 @@
 
     for d in range(1, reach + 1):
         pl.when(level + d < groups)(lambda d=d: z_copy(d).start())
-    for far in range(1, plane):
+    for far in spans:
         pl.when(wanted(0, far, True))(lambda far=far: p_copy(0, far).start())
 
     for copy in loads[3:10]:
@@ -451,7 +451,7 @@
     metas[level] = meta[level]
 
     def m_copy(k):
-        other = nearest(level, groups, k)
+        other = chosen(TARGETS, level, k)
         return remote(
             meta.at[other], metas.at[level], m_send.at[k], m_recv.at[level],
             (other * plane + place, core),
@@ -539,8 +539,8 @@
             t_copy(d, 0, core).start()
 
         pl.when(level >= d)(arrived)
-        for far in range(1, plane):
-            pl.when(wanted(d, far, True))(lambda: p_copy(d, far).start())
+        for far in spans:
+            pl.when(wanted(d, far, True))(lambda far=far: p_copy(d, far).start())
 
     relay(1)
 
@@ -548,8 +548,9 @@
         below = t > place
         turn_at = jnp.where(below, t - place - 1, 0)
         d = jnp.where(below, 1 + turn_at // plane, 0)
-        far = lax.rem(turn_at, plane)
-        far = jnp.where((d == reach) & (far > 0), place + far, far)
+        at = lax.rem(turn_at, plane)
+        far = jnp.where(d == reach, place + at, at)
+        far = jnp.where(at == 0, 0, jnp.where(odd, far, plane - at))
         far = jnp.where(below, far, t)
         block = (level - d) * plane + lax.rem(place + plane - far, plane)
         return block, d, far

time: 107 us -> 99.3 us (0.928)
  the two profiles are of different devices: /device:TPU:0 before, /device:TPU:29 now
where the time goes in v3:
time: 99.3 us; the launch traced here: 99.1 us
  Pallas kernels  97.3 us (98%)
  local copies, waits for them, and re-layouts  1.88 us (2%)
    pallas_call x1, Pallas kernels, layer(): pl.pallas_call(functools.partial(layer_kernel, GROUPS, plane, heads), out...  97.3 us

profile of v3, /device:TPU:29, one launch (start us, length us, event | category | flops | bytes accessed | tf_op | source)
XLA Modules:
  0.0 99.1 jit_solution(463208858321552547)
XLA Ops:
  0.0 97.3 %layer.1 = bf16[128,2048]{1,0:T(8,128)(2,1)} custom-call(bf16[576,256]{1,0:T(8,128)(2,1)} %bitcast.13, bf16[256,256]{1,0:T(8,128)(2,1)} %latent_hbm.1, bf16[32,256]{1,0:T(8,128)(2,1)} %bitcast.14, bf16[256,384]{1,0:T(8,128)(2,1)} %wk_hbm.1, bf16[256,384]{1,0:T(8,128)(2,1)} %wv_hbm.1, bf16[768,2048]{1,0:T(8,128)(2,1)} %proj_hbm.1, ...), custom_call_target="tpu_custom_call" | custom-call | tf_op jit(solution)/shard_map/layer/pallas_call | solution.py:692
  97.3 1.9 %copy.17 = bf16[128,2048]{1,0:T(8,128)(2,1)} copy(bf16[128,2048]{1,0:T(8,128)(2,1)} %layer.1) | data formatting | bytes 1048576

commit v4 on v3

--- a/solution.py
+++ b/solution.py
@@ -17,7 +17,8 @@
 PARTS = 2
 SOURCES = ((0, 1, 3, 2), (1, 0, 2, 3), (2, 0, 1, 3), (3, 0, 1, 2))
 TARGETS = ((0, 1, 3, 2), (1, 2, 3, 0), (2, 1, 0, 3), (3, 0, 1, 2))
-LOWER = ["out1 over0 ffn0 out2", "over1 ffn1 out3 over2", "ffn2 back2 over3 ffn3", "back3 back1 back0 comb2", "comb3 comb1 comb0"]
+LOWEST = ["out1 over0 ffn0 out2", "over1 ffn1 out3 over2", "ffn2 back2 over3 ffn3", "comb2 back3 back1 back0", "comb3 comb1 comb0"]
+LOWER = ["out1 over0 ffn0 over1", "back0 ffn1 out2 out3", "over2 ffn2 back2 over3", "ffn3 comb2 back3 back1", "comb3 comb1 comb0"]
 UPPER = ["out1 out2 over0 ffn0", "over1 ffn1 back1 out3", "over2 ffn2 back2 comb1", "over3 ffn3 back3 back0", "comb2 comb3 comb0"]
 MESH = pl.DeviceIdType.MESH
 
@@ -82,7 +83,7 @@
 
 
 def expert_stage(
-    groups, plane, where, ready, grouped, metas, out_ref,
+    groups, plane, where, ready, settle_sends, conclude, grouped, metas, out_ref,
     gate, up, down, landed, spread, arrived, hidden, partial, passed, mixed, back, merged,
     m_send, m_recv, z_send, z_recv, p_send, p_recv, own_sem, t_send, t_recv,
     x_send, x_recv, b_send, b_recv, keep_sem, r_send, r_recv,
@@ -266,16 +267,24 @@
     def finish(order):
         for name in " ".join(order).split():
             staged(name)
+        for copy in started[: -2 * PARTS]:
+            copy.wait_send()
+        for k in range(groups):
+            if k:
+                z_copy(k).wait_send()
+            for copy in out_copies(k):
+                copy.wait_send()
         with jax.named_scope("E_rest"):
-            for k in range(1, groups):
-                other = source_of[k]
-                for part in range(PARTS):
-                    at = k * PARTS + part
+            for part in range(PARTS):
+                for k in range(1, groups):
+                    other = source_of[k]
                     remote(
                         merged.at[k, part], out_ref.at[other, :, part * cut : (part + 1) * cut],
-                        r_send.at[at], r_recv.at[other * PARTS + part], (other * plane + place, core),
+                        r_send.at[k * PARTS + part], r_recv.at[other * PARTS + part],
+                        (other * plane + place, core),
                     ).wait_recv()
-        for copy in started:
+                conclude(part)
+        for copy in started[-2 * PARTS :]:
             copy.wait_send()
         started.clear()
 
@@ -285,13 +294,10 @@
             z_copy(k).start()
         else:
             staged("out0")
-    pl.when(level < groups // 2)(lambda: finish(LOWER))
+    settle_sends()
+    pl.when(level == 0)(lambda: finish(LOWEST))
+    pl.when((level > 0) & (level < groups // 2))(lambda: finish(LOWER))
     pl.when(level >= groups // 2)(lambda: finish(UPPER))
-    for k in range(groups):
-        if k:
-            z_copy(k).wait_send()
-        for copy in out_copies(k):
-            copy.wait_send()
 
 
 def assign(groups, plane, expert_ids, route, meta_ref):
@@ -352,9 +358,9 @@
     ids_hbm, docs_hbm, route_hbm, mix_gain_hbm, moe_gain_hbm, gate_hbm, up_hbm, down_hbm,
     out_ref,
     query, latent, rope, wk, wv, proj, residual, expert_ids, doc_ids, route, mix_gain, moe_gain,
-    gate, up, down, middle, chooser, returned,
+    gate, up, down, middle, chooser, returned, spots, total_out,
     packs, turned, wv_turned, high, total, acc, halves, full, mix, normed, grouped, meta, metas,
-    load_sem, z_send, z_recv, p_send, p_recv, t_send, t_recv, x_send, x_recv, m_send, m_recv, *rest,
+    load_sem, o_sem, z_send, z_recv, p_send, p_recv, t_send, t_recv, x_send, x_recv, m_send, m_recv, *rest,
 ):
     loads = [
         pltpu.make_async_copy(source, target, load_sem.at[i])
@@ -633,32 +639,44 @@
                 picks, normed[:, columns], preferred_element_type=jnp.float32
             ).astype(jnp.bfloat16)
 
+    spots[...] = chooser[...].astype(jnp.float32).T.astype(jnp.bfloat16)
+    cut = width // PARTS
+
+    def out_copy(part):
+        columns = slice(part * cut, (part + 1) * cut)
+        return pltpu.make_async_copy(total_out.at[part], out_ref.at[:, columns], o_sem.at[part])
+
+    def conclude(part):
+        columns = slice(part * cut, (part + 1) * cut)
+        blended = jnp.dot(
+            spots[...], returned[:, :, columns].reshape(slots, cut), preferred_element_type=jnp.float32
+        )
+        total_out[part] = (middle[:, columns].astype(jnp.float32) + blended).astype(jnp.bfloat16)
+        out_copy(part).start()
+
+    def settle_sends():
+        swap.wait_send()
+        for d in range(reach + 1):
+            for far in range(0 if d else 1, plane):
+                pl.when((level >= d) if far == 0 else wanted(d, far, False))(
+                    lambda d=d, far=far: t_copy(d, far, core).wait_send()
+                )
+                if far:
+                    pl.when(wanted(d, far, True))(lambda d=d, far=far: p_copy(d, far).wait_send())
+        for d in range(1, reach + 1):
+            pl.when(level + d < groups)(lambda d=d: z_copy(d).wait_send())
+        for k in range(1, groups):
+            m_copy(k).wait_send()
+
     for copy in loads[12:]:
         copy.wait()
     expert_stage(
-        groups, plane, (index, core, level, place), ready, grouped, metas, returned,
+        groups, plane, (index, core, level, place), ready, settle_sends, conclude, grouped, metas, returned,
         gate, up, down, *rest[:9], m_send, m_recv, *rest[9:],
     )
 
-    spots = chooser[...].astype(jnp.float32).T.astype(jnp.bfloat16)
-    for j in range(width // tile):
-        columns = slice(j * tile, (j + 1) * tile)
-        mixed = jnp.dot(
-            spots, returned[:, :, columns].reshape(slots, tile), preferred_element_type=jnp.float32
-        )
-        out_ref[:, columns] = (middle[:, columns].astype(jnp.float32) + mixed).astype(jnp.bfloat16)
-    swap.wait_send()
-    for d in range(reach + 1):
-        for far in range(0 if d else 1, plane):
-            pl.when((level >= d) if far == 0 else wanted(d, far, False))(
-                lambda d=d, far=far: t_copy(d, far, core).wait_send()
-            )
-            if far:
-                pl.when(wanted(d, far, True))(lambda d=d, far=far: p_copy(d, far).wait_send())
-    for d in range(1, reach + 1):
-        pl.when(level + d < groups)(lambda d=d: z_copy(d).wait_send())
-    for k in range(1, groups):
-        m_copy(k).wait_send()
+    for part in range(PARTS):
+        out_copy(part).wait()
 
 
 def layer(
@@ -674,7 +692,6 @@
     units = gate.shape[1]
     group_rows = half // 2
     cut = width // PARTS
-    vmem = pl.BlockSpec(memory_space=pltpu.VMEM)
     hbm = pl.BlockSpec(memory_space=pltpu.HBM)
     dma = pltpu.SemaphoreType.DMA
     few, many = dma((GROUPS,)), dma((GROUPS * plane,))
@@ -693,9 +710,10 @@
         functools.partial(layer_kernel, GROUPS, plane, heads),
         out_shape=jax.ShapeDtypeStruct((half, width), jnp.bfloat16),
         in_specs=[hbm] * len(loaded),
-        out_specs=vmem,
+        out_specs=hbm,
         scratch_shapes=[held(*array.shape, dtype=array.dtype) for array in loaded] + [
             held(half, width), held(GROUPS * group_rows, half), held(GROUPS, group_rows, width),
+            held(half, GROUPS * group_rows), held(PARTS, half, cut),
             held(count, 2, half + ROPE, rank),
             held(heads, HEAD_LANES, rows),
             held(heads * VALUE_ENTRIES, rank),
@@ -707,7 +725,7 @@
             held(half, width, dtype=jnp.float32),
             held(half, width),
             held(GROUPS, group_rows, width), table, table,
-            dma((len(loaded),)), few, few, many, many, many, many, dma, dma, few, few,
+            dma((len(loaded),)), dma((PARTS,)), few, few, many, many, many, many, dma, dma, few, few,
             held(GROUPS, group_rows, width),
             held(GROUPS, plane, capacity, width),
             held(GROUPS, 2, plane, capacity, width),

time: 99.3 us -> 98.5 us (level)
  the two profiles are of different devices: /device:TPU:29 before, /device:TPU:16 now
where the time goes in v4:
time: 98.5 us; the launch traced here: 98.4 us
  Pallas kernels  96.5 us (98%)
  local copies, waits for them, and re-layouts  1.88 us (2%)
    pallas_call x1, Pallas kernels, layer(): pl.pallas_call(functools.partial(layer_kernel, GROUPS, plane, heads), out...  96.5 us

profile of v4, /device:TPU:16, one launch (start us, length us, event | category | flops | bytes accessed | tf_op | source)
XLA Modules:
  0.0 98.4 jit_solution(18070134904079066649)
XLA Ops:
  0.0 96.5 %layer.1 = bf16[128,2048]{1,0:T(8,128)(2,1)} custom-call(bf16[576,256]{1,0:T(8,128)(2,1)} %bitcast.13, bf16[256,256]{1,0:T(8,128)(2,1)} %latent_hbm.1, bf16[32,256]{1,0:T(8,128)(2,1)} %bitcast.14, bf16[256,384]{1,0:T(8,128)(2,1)} %wk_hbm.1, bf16[256,384]{1,0:T(8,128)(2,1)} %wv_hbm.1, bf16[768,2048]{1,0:T(8,128)(2,1)} %proj_hbm.1, ...), custom_call_target="tpu_custom_call" | custom-call | tf_op jit(solution)/shard_map/layer/pallas_call | solution.py:709
  96.5 1.9 %copy.17 = bf16[128,2048]{1,0:T(8,128)(2,1)} copy(bf16[128,2048]{1,0:T(8,128)(2,1)} %layer.1) | data formatting | bytes 1048576
